TPU v7x, 32 devices: a whole 2x2x4 slice. The times are simulated.
32 devices in a mesh: ep: 8 (over z, y), tp: 4 (over x, core).
Axes of the slice: x: 2, y: 2, z: 4, core: 2. Of those that a mesh axis runs over, the one named last changes fastest.
Arguments:
- tokens: bfloat16 [64, 1024], P('ep'), may hold values from -6 to 6
- mix_gain: float32 [1024], replicated, may hold values from 0.1 to 1.9
- w_query: bfloat16 [1024, 512], P(None, 'tp'), may hold values from -0.1875 to 0.1875
- w_key: bfloat16 [1024, 512], P(None, 'tp'), may hold values from -0.1875 to 0.1875
- w_value: bfloat16 [1024, 1024], P(None, 'tp'), may hold values from -0.1875 to 0.1875
- w_ogate: bfloat16 [1024, 1024], P(None, 'tp'), may hold values from -0.1875 to 0.1875
- w_igate: bfloat16 [1024, 4], replicated, may hold values from -0.1875 to 0.1875
- w_fgate: bfloat16 [1024, 4], replicated, may hold values from -0.1875 to 0.1875
- forget_bias: float32 [4], replicated, may hold values from -1 to 3
- head_gain: float32 [1024], P('tp'), may hold values from 0.1 to 1.9
- w_out: bfloat16 [1024, 1024], P('tp'), may hold values from -0.1875 to 0.1875
- memory: float32 [64, 4, 128, 256], P('ep', 'tp'), may hold values from -0.4 to 0.4
- normalizer: float32 [64, 4, 128], P('ep', 'tp'), may hold values from -0.4 to 0.4
- running_max: float32 [64, 4], P('ep', 'tp'), may hold values from -4 to 4
- ffn_gain: float32 [1024], replicated, may hold values from 0.1 to 1.9
- route: int32 [64, 2], replicated, may hold values from 0 to 7, all different within a row; in each aligned block of 64 rows (0 to 63, 64 to 127, ...) at most 32 rows name the same one
- route_weight: float32 [64, 2], replicated, may hold values from 0.05 to 1
- w_gate: bfloat16 [8, 1024, 512], P('ep', None, 'tp'), may hold values from -0.1875 to 0.1875
- w_up: bfloat16 [8, 1024, 512], P('ep', None, 'tp'), may hold values from -0.1875 to 0.1875
- w_down: bfloat16 [8, 512, 1024], P('ep', 'tp'), may hold values from -0.25 to 0.25
Outputs:
- mixed: bfloat16 [64, 1024], P(None, 'ep')
- new_memory: float32 [64, 4, 128, 256], P('ep', 'tp')
- new_normalizer: float32 [64, 4, 128], P('ep', 'tp')
- new_max: float32 [64, 4], P('ep', 'tp')
Inputs may be any that keep to these rules, and one draw needn't show every extreme that they name: `route`: each expert is named by at most 32 routes in all, a bound that some block reaches; the two choices of a token differ.
All inputs are finite; a program needn't handle non-finite values.
Results may differ from a plain program's by a relative error of at most 0.014.
Values may be sent and summed in bfloat16 or wider, within the bound.
No kernel may reach another device: no remote copies, remote signals or barrier semaphores. Data moves between devices by JAX's collectives and lax.ppermute only.
A program may use at most 64 MiB of HBM per device.

v0:
```python
import jax
import jax.numpy as jnp
from jax import lax
from jax.sharding import PartitionSpec as P

EXPERT_CAPACITY = 32
EPS = 1e-06


def round_trip(values):
    rounded = lax.optimization_barrier(values.astype(jnp.bfloat16))
    return rounded.astype(jnp.float32)


def norm_rows(values, gain):
    floats = values.astype(jnp.float32)
    scale = lax.rsqrt(jnp.mean(floats * floats, axis=-1, keepdims=True) + EPS)
    return (floats * scale * gain).astype(jnp.bfloat16)


def slot_targets(route, expert_count, capacity):
    flat = route.reshape(-1)
    onehot = (flat[:, None] == jnp.arange(expert_count, dtype=jnp.int32)[None, :]).astype(jnp.int32)
    before = jnp.cumsum(onehot, axis=0) - onehot
    slot = jnp.sum(before * onehot, axis=1)
    return flat * capacity + slot


def shards(
    tokens,
    mix_gain,
    w_query,
    w_key,
    w_value,
    w_ogate,
    w_igate,
    w_fgate,
    forget_bias,
    head_gain,
    w_out,
    memory,
    normalizer,
    running_max,
    ffn_gain,
    route,
    route_weight,
    w_gate,
    w_up,
    w_down,
):
    width = tokens.shape[1]
    col_count = width // lax.axis_size("ep")
    qk_dim = w_query.shape[1]
    normed = norm_rows(tokens, mix_gain)
    query = round_trip(jnp.dot(normed, w_query, preferred_element_type=jnp.float32))
    scaled_key = round_trip(
        jnp.dot(normed, w_key, preferred_element_type=jnp.float32)
    ) * qk_dim ** (-0.5)
    value = round_trip(jnp.dot(normed, w_value, preferred_element_type=jnp.float32))
    ogate = round_trip(jnp.dot(normed, w_ogate, preferred_element_type=jnp.float32))
    head_pick = (jnp.arange(w_igate.shape[1], dtype=jnp.int32) == lax.axis_index("tp")).astype(
        jnp.float32
    )
    log_in = jnp.sum(
        jnp.dot(normed, w_igate, preferred_element_type=jnp.float32) * head_pick, axis=1
    )
    forget_pre = jnp.sum(
        jnp.dot(normed, w_fgate, preferred_element_type=jnp.float32) * head_pick, axis=1
    )
    log_forget = jax.nn.log_sigmoid(forget_pre + jnp.sum(forget_bias * head_pick))
    old_max = running_max[:, 0]
    new_max = jnp.maximum(log_forget + old_max, log_in)
    keep = jnp.exp(log_forget + old_max - new_max)
    admit = jnp.exp(log_in - new_max)
    state = (
        keep[:, None, None] * memory[:, 0]
        + admit[:, None, None] * scaled_key[:, :, None] * value[:, None, :]
    )
    norm_state = keep[:, None] * normalizer[:, 0] + admit[:, None] * scaled_key
    numer = jnp.einsum("tk,tkv->tv", query, state, precision=lax.Precision.HIGHEST)
    denom = jnp.sum(query * norm_state, axis=1)
    read = numer / jnp.maximum(jnp.abs(denom), jnp.exp(-new_max))[:, None]
    scale = lax.rsqrt(jnp.mean(read * read, axis=-1, keepdims=True) + EPS)
    gated = (jax.nn.sigmoid(ogate) * read * scale * head_gain).astype(jnp.bfloat16)
    local_output = lax.psum(
        jnp.dot(gated, w_out, preferred_element_type=jnp.float32).astype(jnp.bfloat16), "tp"
    ).astype(jnp.float32)
    middle_rows = (tokens.astype(jnp.float32) + local_output).astype(jnp.bfloat16)
    middle = lax.all_to_all(middle_rows, "ep", split_axis=1, concat_axis=0, tiled=True)
    expert_count = w_gate.shape[0] * lax.axis_size("ep")
    topk_count = route.shape[1]
    targets = slot_targets(route, expert_count, EXPERT_CAPACITY)
    buffer = (
        jnp.zeros((expert_count * EXPERT_CAPACITY, col_count), jnp.bfloat16)
        .at[targets]
        .set(jnp.repeat(middle, topk_count, axis=0))
    )
    buffer = buffer.reshape(expert_count, EXPERT_CAPACITY, col_count)
    rows = lax.all_to_all(buffer, "ep", split_axis=0, concat_axis=2, tiled=True)
    rows = norm_rows(rows, ffn_gain)
    gate_v = jnp.einsum("ecd,edf->ecf", rows, w_gate, preferred_element_type=jnp.float32)
    up_v = jnp.einsum("ecd,edf->ecf", rows, w_up, preferred_element_type=jnp.float32)
    activation = (jax.nn.silu(gate_v) * up_v).astype(jnp.bfloat16)
    partial_value = jnp.einsum(
        "ecf,efd->ecd", activation, w_down, preferred_element_type=jnp.float32
    )
    results = lax.psum(partial_value.astype(jnp.bfloat16), "tp")
    returned = lax.all_to_all(results, "ep", split_axis=2, concat_axis=0, tiled=True)
    picked = returned.reshape(expert_count * EXPERT_CAPACITY, col_count)[targets]
    picked = picked.reshape(route.shape[0], topk_count, col_count).astype(jnp.float32)
    weights = route_weight / jnp.sum(route_weight, axis=1, keepdims=True)
    mixed = (middle.astype(jnp.float32) + jnp.sum(picked * weights[:, :, None], axis=1)).astype(
        jnp.bfloat16
    )
    return (mixed, state[:, None], norm_state[:, None], new_max[:, None])


def solution(mesh):
    return jax.shard_map(
        shards,
        mesh=mesh,
        in_specs=(
            P("ep", None),
            P(),
            P(None, "tp"),
            P(None, "tp"),
            P(None, "tp"),
            P(None, "tp"),
            P(),
            P(),
            P(),
            P("tp"),
            P("tp", None),
            P("ep", "tp", None, None),
            P("ep", "tp", None),
            P("ep", "tp"),
            P(),
            P(),
            P(),
            P("ep", None, "tp"),
            P("ep", None, "tp"),
            P("ep", "tp", None),
        ),
        out_specs=(P(None, "ep"), P("ep", "tp", None, None), P("ep", "tp", None), P("ep", "tp")),
        check_vma=False,
    )
```

profile of v0, /device:TPU:0, one launch (start us, length us, event | category | flops | bytes accessed | tf_op | source)
XLA Modules:
  0.0 114.8 jit_solution(4171381798939121330)
XLA Ops:
  7.2 1.4 %fusion.48 = f32[]{:T(128)} fusion(f32[4]{0:T(128)} %param.28, s32[]{:T(128)S(6)} %axis_index.12), kind=kLoop, calls=%fused_computation.81 | loop fusion | flops 11 | bytes 24 | tf_op jit(solution)/shard_map/reduce_sum | solution.py:70
  8.7 0.8 fusion.28
  9.5 0.9 fusion.3
  10.4 0.9 fusion.2
  11.3 1.3 %fusion.46 = (f32[8]{0:T(128)S(1)}, f32[8]{0:T(128)S(1)}) fusion(f32[8]{0:T(128)S(1)} %fusion.3, f32[8,1]{0,1:T(1,128)} %param.33, f32[8]{0:T(128)S(1)} %fusion.2, f32[]{:T(128)} %fusion.48), kind=kLoop, calls=%fused_computation.79 | loop fusion | flops 96 | bytes 164 | tf_op jit(solution)/shard_map/exp | solution.py:73
  12.7 1.3 %exponential_bitcast_fusion = (f32[8]{0:T(128)S(1)}, f32[8,1]{0,1:T(1,128)S(1)}) fusion(f32[8]{0:T(128)S(1)} %fusion.3, f32[8,1]{0,1:T(1,128)} %param.33, f32[8]{0:T(128)S(1)} %fusion.2, f32[]{:T(128)} %fusion.48), kind=kLoop, calls=%fused_computation.104 | loop fusion | flops 96 | bytes 164 | tf_op jit(solution)/shard_map/mul | solution.py:79
  14.1 0.9 convolution_convert_fusion.5
  14.9 1.2 %convolution_convert_fusion.4 = bf16[8,128]{1,0:T(8,128)(2,1)S(1)} fusion(bf16[1024,128]{1,0:T(8,128)(2,1)} %param.23, bf16[8,1024]{1,0:T(8,128)(2,1)S(1)} %copy-done.3, f32[1024]{0:T(1024)} %param.21, f32[8]{0:T(128)S(1)} %add_rsqrt_fusion.2), kind=kOutput, calls=%fused_computation.9 | convolution fusion | flops 2130944 | bytes 284704 | tf_op jit(solution)/shard_map/dot_general | solution.py:57
  16.1 0.9 convolution_convert_fusion.2
  17.0 1.3 %convolution_convert_fusion.3 = bf16[8,256]{1,0:T(8,128)(2,1)S(1)} fusion(bf16[1024,256]{1,0:T(8,128)(2,1)} %param.25, bf16[8,1024]{1,0:T(8,128)(2,1)S(1)} %copy-done.3, f32[1024]{0:T(1024)} %param.21, f32[8]{0:T(128)S(1)} %add_rsqrt_fusion.2), kind=kOutput, calls=%fused_computation.8 | convolution fusion | flops 4229120 | bytes 548896 | tf_op jit(solution)/shard_map/dot_general | solution.py:60
  19.0 0.8 multiply_reduce_fusion.1
  21.5 12.7 %psum.14 = bf16[8,1024]{1,0:T(8,128)(2,1)S(1)} all-reduce(bf16[8,1024]{1,0:T(8,128)(2,1)S(1)} %convolution_convert_fusion.1), channel_id=1, replica_groups=mesh['ep'=8,'tp'=4] {'tp'}, use_global_device_ids=true, to_apply=%region_6.7 | all-reduce | flops 8192 | bytes 32768 | tf_op jit(solution)/shard_map/psum | solution.py:85
  34.8 6.0 %all-to-all-start = ((bf16[8,8,128]{2,0,1:T(8,128)(2,1)}), bf16[8,8,128]{2,0,1:T(8,128)(2,1)S(1)}, u32[]{:S(2)}, u32[]{:S(2)}) async-start(bf16[8,8,128]{2,0,1:T(8,128)(2,1)} %fusion.34), calls=%async_computation | async-start | bytes 32768 | tf_op jit(solution)/shard_map/all_to_all | solution.py:89
  41.8 5.6 %all-to-all-done = bf16[8,8,128]{2,0,1:T(8,128)(2,1)S(1)} async-done(((bf16[8,8,128]{2,0,1:T(8,128)(2,1)}), bf16[8,8,128]{2,0,1:T(8,128)(2,1)S(1)}, u32[]{:S(2)}, u32[]{:S(2)}) %all-to-all-start) | async-done | bytes 16416 | tf_op jit(solution)/shard_map/all_to_all | solution.py:89
  47.4 0.9 scatter_custom_fusion
  48.3 9.3 %all_to_all.43 = bf16[8,32,128]{2,1,0:T(8,128)(2,1)S(1)} all-to-all(bf16[8,32,128]{2,1,0:T(8,128)(2,1)S(1)} %bitcast.126), channel_id=1, replica_groups=mesh['ep'=8,'tp'=4] {'ep'}, dimensions={0} | all-to-all | bytes 131072 | tf_op jit(solution)/shard_map/all_to_all | solution.py:99
  59.3 0.9 fusion
  60.3 1.2 %multiply_add_fusion = f32[8,1,128,256]{3,2,1,0:T(8,128)} fusion(f32[8,1,128,256]{3,2,1,0:T(8,128)S(1)} %copy-done.1, f32[8,256]{1,0:T(8,128)S(1)} %convert_element_type.117, f32[8,128]{1,0:T(8,128)S(1)} %get-tuple-element.30, f32[8]{0:T(128)S(1)} %get-tuple-element.24), kind=kLoop, calls=%fused_computation.18 | loop fusion | flops 786432 | bytes 2109472 | tf_op jit(solution)/shard_map/add | solution.py:76
  61.5 27.0 %all-reduce.2.cloned.1.call-done = bf16[1,32,1024]{2,1,0:T(8,128)(2,1)} async-done(((bf16[1,32,1024]{2,1,0:T(8,128)(2,1)}), bf16[1,32,1024]{2,1,0:T(8,128)(2,1)}) %all-reduce.2.cloned.1.call-update) | async-done | bytes 65552 | tf_op jit(solution)/shard_map/psum | solution.py:107
  88.5 1.1 copy.50
  90.1 2.3 %reduce.3 = bf16[1024,32]{1,0:T(8,128)(2,1)S(1)} reduce(bf16[1024,1,32]{2,1,0:T(2,128)(2,1)S(1)} %bitcast.121, bf16[]{:T(256)} %broadcast.215), dimensions={1}, to_apply=%bitcast.105.reduce_sub_computation | reduce | bytes 131074
  92.4 0.9 reshape.303
  93.3 5.5 %all-to-all-start.2 = ((bf16[8,2,2048]{2,1,0:T(2,128)(2,1)}), bf16[8,2,2048]{2,1,0:T(2,128)(2,1)S(1)}, u32[]{:S(2)}, u32[]{:S(2)}) async-start(bf16[8,2,2048]{2,1,0:T(2,128)(2,1)} %reshape.303), calls=%async_computation.2 | async-start | bytes 131072 | tf_op jit(solution)/shard_map/all_to_all | solution.py:108
  99.0 6.8 %all-to-all-done.2 = bf16[8,2,2048]{2,1,0:T(2,128)(2,1)S(1)} async-done(((bf16[8,2,2048]{2,1,0:T(2,128)(2,1)}), bf16[8,2,2048]{2,1,0:T(2,128)(2,1)S(1)}, u32[]{:S(2)}, u32[]{:S(2)}) %all-to-all-start.2) | async-done | bytes 65568 | tf_op jit(solution)/shard_map/all_to_all | solution.py:108
  (69 shorter events, 8.5 us)
Async XLA Ops:
  7.2 13.5 %copy-start = (bf16[256,1024]{1,0:T(8,128)(2,1)S(1)}, bf16[256,1024]{1,0:T(8,128)(2,1)}, u32[]{:S(2)}) copy-start(bf16[256,1024]{1,0:T(8,128)(2,1)} %param.30) | copy-start | bytes 1572868
  7.2 2.3 %copy-start.3 = (bf16[8,1024]{1,0:T(8,128)(2,1)S(1)}, bf16[8,1024]{1,0:T(8,128)(2,1)}, u32[]{:S(2)}) copy-start(bf16[8,1024]{1,0:T(8,128)(2,1)} %param.20) | copy-start | bytes 49156
  7.2 6.8 %copy-start.12 = (bf16[1024,128]{1,0:T(8,128)(2,1)S(1)}, bf16[1024,128]{1,0:T(8,128)(2,1)}, u32[]{:S(2)}) copy-start(bf16[1024,128]{1,0:T(8,128)(2,1)} %param.22) | copy-start | bytes 786436
  7.2 8.9 %copy-start.2 = (bf16[1024,256]{1,0:T(8,128)(2,1)S(1)}, bf16[1024,256]{1,0:T(8,128)(2,1)}, u32[]{:S(2)}) copy-start(bf16[1024,256]{1,0:T(8,128)(2,1)} %param.24) | copy-start | bytes 1572868
  7.2 12.6 %copy-start.1 = (f32[8,1,128,256]{3,2,1,0:T(8,128)S(1)}, f32[8,1,128,256]{3,2,1,0:T(8,128)}, u32[]{:S(2)}) copy-start(f32[8,1,128,256]{3,2,1,0:T(8,128)} %param.31) | copy-start | bytes 3145732
  14.0 5.8 %copy-start.11 = (f32[8,1]{0,1:T(1,128)}, f32[8,1]{0,1:T(1,128)S(1)}, u32[]{:S(2)}) copy-start(f32[8,1]{0,1:T(1,128)S(1)} %get-tuple-element.29) | copy-start | bytes 100
  18.3 0.7 copy-start.10
  20.6 0.7 copy-start.13
  34.8 6.0 %copy-start.8 = (s32[64,2]{0,1:T(2,128)S(1)}, s32[64,2]{0,1:T(2,128)}, u32[]{:S(2)}) copy-start(s32[64,2]{0,1:T(2,128)} %param.35) | copy-start | bytes 1540
  34.8 12.5 %all-to-all-start = ((bf16[8,8,128]{2,0,1:T(8,128)(2,1)}), bf16[8,8,128]{2,0,1:T(8,128)(2,1)S(1)}, u32[]{:S(2)}, u32[]{:S(2)}) async-start(bf16[8,8,128]{2,0,1:T(8,128)(2,1)} %fusion.34), calls=%async_computation | async-start | bytes 32768 | tf_op jit(solution)/shard_map/all_to_all | solution.py:89
  40.8 47.7 %all-reduce.2.cloned.1.call-start = ((), (), s32[]{:S(2)}) async-start(), calls=%async_computation.3 | async-start | bytes 131072 | tf_op jit(solution)/shard_map/psum | solution.py:107
  47.4 11.0 %copy-start.4 = (bf16[1,1024,128]{2,1,0:T(8,128)(2,1)S(1)}, bf16[1,1024,128]{2,1,0:T(8,128)(2,1)}, u32[]{:S(2)}) copy-start(bf16[1,1024,128]{2,1,0:T(8,128)(2,1)} %param.37) | copy-start | bytes 786436
  57.6 0.7 copy-start.7
  58.3 0.9 copy-start.6
  58.4 1.0 copy-start.5
  60.3 1.2 %copy-start.9 = (f32[64,2]{0,1:T(2,128)S(1)}, f32[64,2]{0,1:T(2,128)}, u32[]{:S(2)}) copy-start(f32[64,2]{0,1:T(2,128)} %param.36) | copy-start | bytes 1540
  93.3 12.4 %all-to-all-start.2 = ((bf16[8,2,2048]{2,1,0:T(2,128)(2,1)}), bf16[8,2,2048]{2,1,0:T(2,128)(2,1)S(1)}, u32[]{:S(2)}, u32[]{:S(2)}) async-start(bf16[8,2,2048]{2,1,0:T(2,128)(2,1)} %reshape.303), calls=%async_computation.2 | async-start | bytes 131072 | tf_op jit(solution)/shard_map/all_to_all | solution.py:108
Sparse Core Ops, SparseCore 0:
  60.4 28.0 all-reduce.1
where the time goes:
time: 116 us; the launch traced here: 115 us
  waiting for transfers between devices  39.4 us (34%)
  blocking collectives  22 us (19%)
  between operations  14.3 us (12%)
  starting transfers between devices  11.5 us (10%)
  other arithmetic  11.4 us (10%)
  local copies, waits for them, and re-layouts  8.14 us (7%)
  matrix products  7.98 us (7%)
    psum x1, waiting for transfers between devices, shards(): results = lax.psum(partial_value.astype(jnp.bfloat16), 'tp')  27 us
    psum x1, blocking collectives, shards(): lax.psum(jnp.dot(gated, w_out, preferred_element_type=jnp.float32).astype...  12.7 us
    all_to_all x1, blocking collectives, shards(): rows = lax.all_to_all(buffer, 'ep', split_axis=0, concat_axis=2, tiled=True)  9.29 us
    all_to_all x1, waiting for transfers between devices, shards(): lax.all_to_all(results, 'ep', split_axis=2, concat_axis=0, tiled=True)  6.79 us
    all_to_all x1, starting transfers between devices, shards(): lax.all_to_all(middle_rows, 'ep', split_axis=1, concat_axis=0, tiled=True)  5.97 us
    all_to_all x1, waiting for transfers between devices, shards(): lax.all_to_all(middle_rows, 'ep', split_axis=1, concat_axis=0, tiled=True)  5.58 us
    all_to_all x1, starting transfers between devices, shards(): lax.all_to_all(results, 'ep', split_axis=2, concat_axis=0, tiled=True)  5.52 us
    unnamed x33, local copies, waits for them, and re-layouts  4.59 us
  transfers between devices with their start and end apart: 3, of which 3 were waited for; matrix products, arithmetic and copies ran while one was open for 2% of the time, Pallas kernels for 0%

commit v1 on v0

--- a/solution.py
+++ b/solution.py
@@ -86,7 +86,10 @@
         jnp.dot(gated, w_out, preferred_element_type=jnp.float32).astype(jnp.bfloat16), "tp"
     ).astype(jnp.float32)
     middle_rows = (tokens.astype(jnp.float32) + local_output).astype(jnp.bfloat16)
-    middle = lax.all_to_all(middle_rows, "ep", split_axis=1, concat_axis=0, tiled=True)
+    middle = jnp.concatenate(
+        lax.all_to_all(jnp.stack(jnp.split(middle_rows, lax.axis_size("ep"), axis=1)), "ep", 0, 0),
+        axis=0,
+    )
     expert_count = w_gate.shape[0] * lax.axis_size("ep")
     topk_count = route.shape[1]
     targets = slot_targets(route, expert_count, EXPERT_CAPACITY)

time: 116 us -> 120 us (1.034)
  local copies, waits for them, and re-layouts: 8.14 us -> 12.8 us
    unnamed x33 -> x40, local copies, waits for them, and re-layouts: 4.59 us -> 8.64 us
where the time goes in v1:
time: 120 us; the launch traced here: 119 us
  waiting for transfers between devices  39.4 us (33%)
  blocking collectives  22 us (18%)
  between operations  14.3 us (12%)
  local copies, waits for them, and re-layouts  12.8 us (11%)
  starting transfers between devices  11.5 us (10%)
  other arithmetic  10.8 us (9%)
  matrix products  7.98 us (7%)
    psum x1, waiting for transfers between devices, shards(): results = lax.psum(partial_value.astype(jnp.bfloat16), 'tp')  27 us
    psum x1, blocking collectives, shards(): lax.psum(jnp.dot(gated, w_out, preferred_element_type=jnp.float32).astype...  12.7 us
    all_to_all x1, blocking collectives, shards(): rows = lax.all_to_all(buffer, 'ep', split_axis=0, concat_axis=2, tiled=True)  9.29 us
    unnamed x40, local copies, waits for them, and re-layouts  8.64 us
    all_to_all x1, waiting for transfers between devices, shards(): lax.all_to_all(results, 'ep', split_axis=2, concat_axis=0, tiled=True)  6.79 us
    all_to_all x1, starting transfers between devices, shards(): lax.all_to_all(jnp.stack(jnp.split(middle_rows, lax.axis_size('ep'), axis...  5.97 us
    all_to_all x1, waiting for transfers between devices, shards(): lax.all_to_all(jnp.stack(jnp.split(middle_rows, lax.axis_size('ep'), axis...  5.58 us
    all_to_all x1, starting transfers between devices, shards(): lax.all_to_all(results, 'ep', split_axis=2, concat_axis=0, tiled=True)  5.52 us
  transfers between devices with their start and end apart: 3, of which 3 were waited for; matrix products, arithmetic and copies ran while one was open for 2% of the time, Pallas kernels for 0%

profile of v1, /device:TPU:0, one launch (start us, length us, event | category | flops | bytes accessed | tf_op | source)
XLA Modules:
  0.0 118.8 jit_solution(5787094880206951014)
XLA Ops:
  7.2 1.4 %fusion.47 = f32[]{:T(128)} fusion(f32[4]{0:T(128)} %param.28, s32[]{:T(128)S(6)} %axis_index.12), kind=kLoop, calls=%fused_computation.96 | loop fusion | flops 11 | bytes 24 | tf_op jit(solution)/shard_map/reduce_sum | solution.py:70
  8.7 0.8 fusion.28
  9.5 0.9 fusion.3
  10.4 0.9 fusion.2
  11.3 1.3 %fusion.45 = (f32[8]{0:T(128)S(1)}, f32[8]{0:T(128)S(1)}) fusion(f32[8]{0:T(128)S(1)} %fusion.3, f32[8,1]{0,1:T(1,128)} %param.33, f32[8]{0:T(128)S(1)} %fusion.2, f32[]{:T(128)} %fusion.47), kind=kLoop, calls=%fused_computation.94 | loop fusion | flops 96 | bytes 164 | tf_op jit(solution)/shard_map/exp | solution.py:73
  12.7 1.3 %exponential_bitcast_fusion = (f32[8]{0:T(128)S(1)}, f32[8,1]{0,1:T(1,128)S(1)}) fusion(f32[8]{0:T(128)S(1)} %fusion.3, f32[8,1]{0,1:T(1,128)} %param.33, f32[8]{0:T(128)S(1)} %fusion.2, f32[]{:T(128)} %fusion.47), kind=kLoop, calls=%fused_computation.119 | loop fusion | flops 96 | bytes 164 | tf_op jit(solution)/shard_map/mul | solution.py:79
  14.1 0.9 convolution_convert_fusion.5
  14.9 1.2 convolution_convert_fusion.4
  16.1 0.9 convolution_convert_fusion.2
  17.0 1.3 %convolution_convert_fusion.3 = bf16[8,256]{1,0:T(8,128)(2,1)S(1)} fusion(bf16[1024,256]{1,0:T(8,128)(2,1)} %param.25, bf16[8,1024]{1,0:T(8,128)(2,1)S(1)} %copy-done.3, f32[1024]{0:T(1024)} %param.21, f32[8]{0:T(128)S(1)} %add_rsqrt_fusion.2), kind=kOutput, calls=%fused_computation.8 | convolution fusion | flops 4229120 | bytes 548896 | tf_op jit(solution)/shard_map/dot_general | solution.py:60
  19.0 0.8 multiply_reduce_fusion.1
  21.5 12.7 %psum.14 = bf16[8,1024]{1,0:T(8,128)(2,1)S(1)} all-reduce(bf16[8,1024]{1,0:T(8,128)(2,1)S(1)} %convolution_convert_fusion.1), channel_id=1, replica_groups=mesh['ep'=8,'tp'=4] {'tp'}, use_global_device_ids=true, to_apply=%region_6.7 | all-reduce | flops 8192 | bytes 32768 | tf_op jit(solution)/shard_map/psum | solution.py:85
  38.8 6.0 %all-to-all-start = ((bf16[8,8,128]{2,1,0:T(8,128)(2,1)}), bf16[8,8,128]{2,1,0:T(8,128)(2,1)S(1)}, u32[]{:S(2)}, u32[]{:S(2)}) async-start(bf16[8,8,128]{2,1,0:T(8,128)(2,1)} %constant_dynamic-update-slice_fusion), calls=%async_computation | async-start | bytes 32768 | tf_op jit(solution)/shard_map/all_to_all | solution.py:90
  45.8 5.6 %all-to-all-done = bf16[8,8,128]{2,1,0:T(8,128)(2,1)S(1)} async-done(((bf16[8,8,128]{2,1,0:T(8,128)(2,1)}), bf16[8,8,128]{2,1,0:T(8,128)(2,1)S(1)}, u32[]{:S(2)}, u32[]{:S(2)}) %all-to-all-start) | async-done | bytes 16416 | tf_op jit(solution)/shard_map/all_to_all | solution.py:90
  51.4 0.9 scatter_custom_fusion
  52.3 9.3 %all_to_all.29 = bf16[8,32,128]{2,1,0:T(8,128)(2,1)S(1)} all-to-all(bf16[8,32,128]{2,1,0:T(8,128)(2,1)S(1)} %bitcast.154), channel_id=1, replica_groups=mesh['ep'=8,'tp'=4] {'ep'}, dimensions={0} | all-to-all | bytes 131072 | tf_op jit(solution)/shard_map/all_to_all | solution.py:102
  63.4 0.9 fusion
  64.3 1.2 multiply_add_fusion
  65.5 27.0 %all-reduce.2.cloned.1.call-done = bf16[1,32,1024]{2,1,0:T(8,128)(2,1)} async-done(((bf16[1,32,1024]{2,1,0:T(8,128)(2,1)}), bf16[1,32,1024]{2,1,0:T(8,128)(2,1)}) %all-reduce.2.cloned.1.call-update) | async-done | bytes 65552 | tf_op jit(solution)/shard_map/psum | solution.py:110
  92.5 1.1 copy.50
  94.2 2.3 %reduce.3 = bf16[1024,32]{1,0:T(8,128)(2,1)S(1)} reduce(bf16[1024,1,32]{2,1,0:T(2,128)(2,1)S(1)} %bitcast.149, bf16[]{:T(256)} %broadcast.215), dimensions={1}, to_apply=%bitcast.133.reduce_sub_computation | reduce | bytes 131074
  96.5 0.9 reshape.304
  97.4 5.5 %all-to-all-start.2 = ((bf16[8,2,2048]{2,1,0:T(2,128)(2,1)}), bf16[8,2,2048]{2,1,0:T(2,128)(2,1)S(1)}, u32[]{:S(2)}, u32[]{:S(2)}) async-start(bf16[8,2,2048]{2,1,0:T(2,128)(2,1)} %reshape.304), calls=%async_computation.2 | async-start | bytes 131072 | tf_op jit(solution)/shard_map/all_to_all | solution.py:111
  103.0 6.8 %all-to-all-done.2 = bf16[8,2,2048]{2,1,0:T(2,128)(2,1)S(1)} async-done(((bf16[8,2,2048]{2,1,0:T(2,128)(2,1)}), bf16[8,2,2048]{2,1,0:T(2,128)(2,1)S(1)}, u32[]{:S(2)}, u32[]{:S(2)}) %all-to-all-start.2) | async-done | bytes 65568 | tf_op jit(solution)/shard_map/all_to_all | solution.py:111
  (77 shorter events, 12.6 us)
Async XLA Ops:
  7.2 13.5 %copy-start = (bf16[256,1024]{1,0:T(8,128)(2,1)S(1)}, bf16[256,1024]{1,0:T(8,128)(2,1)}, u32[]{:S(2)}) copy-start(bf16[256,1024]{1,0:T(8,128)(2,1)} %param.30) | copy-start | bytes 1572868
  7.2 2.3 %copy-start.3 = (bf16[8,1024]{1,0:T(8,128)(2,1)S(1)}, bf16[8,1024]{1,0:T(8,128)(2,1)}, u32[]{:S(2)}) copy-start(bf16[8,1024]{1,0:T(8,128)(2,1)} %param.20) | copy-start | bytes 49156
  7.2 6.8 %copy-start.12 = (bf16[1024,128]{1,0:T(8,128)(2,1)S(1)}, bf16[1024,128]{1,0:T(8,128)(2,1)}, u32[]{:S(2)}) copy-start(bf16[1024,128]{1,0:T(8,128)(2,1)} %param.22) | copy-start | bytes 786436
  7.2 8.9 %copy-start.2 = (bf16[1024,256]{1,0:T(8,128)(2,1)S(1)}, bf16[1024,256]{1,0:T(8,128)(2,1)}, u32[]{:S(2)}) copy-start(bf16[1024,256]{1,0:T(8,128)(2,1)} %param.24) | copy-start | bytes 1572868
  7.2 12.6 %copy-start.1 = (f32[8,1,128,256]{3,2,1,0:T(8,128)S(1)}, f32[8,1,128,256]{3,2,1,0:T(8,128)}, u32[]{:S(2)}) copy-start(f32[8,1,128,256]{3,2,1,0:T(8,128)} %param.31) | copy-start | bytes 3145732
  14.0 5.8 %copy-start.11 = (f32[8,1]{0,1:T(1,128)}, f32[8,1]{0,1:T(1,128)S(1)}, u32[]{:S(2)}) copy-start(f32[8,1]{0,1:T(1,128)S(1)} %get-tuple-element.29) | copy-start | bytes 100
  18.3 0.7 copy-start.10
  20.6 0.7 copy-start.13
  38.8 6.0 %copy-start.8 = (s32[64,2]{0,1:T(2,128)S(1)}, s32[64,2]{0,1:T(2,128)}, u32[]{:S(2)}) copy-start(s32[64,2]{0,1:T(2,128)} %param.35) | copy-start | bytes 1540
  38.8 12.5 %all-to-all-start = ((bf16[8,8,128]{2,1,0:T(8,128)(2,1)}), bf16[8,8,128]{2,1,0:T(8,128)(2,1)S(1)}, u32[]{:S(2)}, u32[]{:S(2)}) async-start(bf16[8,8,128]{2,1,0:T(8,128)(2,1)} %constant_dynamic-update-slice_fusion), calls=%async_computation | async-start | bytes 32768 | tf_op jit(solution)/shard_map/all_to_all | solution.py:90
  44.8 47.7 %all-reduce.2.cloned.1.call-start = ((), (), s32[]{:S(2)}) async-start(), calls=%async_computation.3 | async-start | bytes 131072 | tf_op jit(solution)/shard_map/psum | solution.py:110
  51.4 11.0 %copy-start.4 = (bf16[1,1024,128]{2,1,0:T(8,128)(2,1)S(1)}, bf16[1,1024,128]{2,1,0:T(8,128)(2,1)}, u32[]{:S(2)}) copy-start(bf16[1,1024,128]{2,1,0:T(8,128)(2,1)} %param.37) | copy-start | bytes 786436
  61.6 0.7 copy-start.7
  62.3 0.9 copy-start.6
  62.4 1.0 copy-start.5
  64.3 1.2 %copy-start.9 = (f32[64,2]{0,1:T(2,128)S(1)}, f32[64,2]{0,1:T(2,128)}, u32[]{:S(2)}) copy-start(f32[64,2]{0,1:T(2,128)} %param.36) | copy-start | bytes 1540
  97.4 12.4 %all-to-all-start.2 = ((bf16[8,2,2048]{2,1,0:T(2,128)(2,1)}), bf16[8,2,2048]{2,1,0:T(2,128)(2,1)S(1)}, u32[]{:S(2)}, u32[]{:S(2)}) async-start(bf16[8,2,2048]{2,1,0:T(2,128)(2,1)} %reshape.304), calls=%async_computation.2 | async-start | bytes 131072 | tf_op jit(solution)/shard_map/all_to_all | solution.py:111
Sparse Core Ops, SparseCore 0:
  64.4 28.0 all-reduce.1
